TPU v7x, 256 devices: a whole 4x4x8 slice. The times are simulated.
256 devices in a mesh: ep: 128 (over z, y, x), tp: 2 (over core).
Axes of the slice: x: 4, y: 4, z: 8, core: 2. Of those that a mesh axis runs over, the one named last changes fastest.
Arguments:
- tokens: bfloat16 [8192, 1024], P('ep', 'tp'), may hold values from -6 to 6
- norm_gain: float32 [1024], P('tp'), may hold values from 0.1 to 1.9
- routing: int32 [8192, 2], P('ep'), may hold values from 0 to 255, as said below
- route_weight: float32 [8192, 2], P('ep'), may hold values from 0.25 to 1
- w_gate: bfloat16 [256, 1024, 512], P('ep', None, 'tp'), may hold values from -0.1875 to 0.1875
- w_up: bfloat16 [256, 1024, 512], P('ep', None, 'tp'), may hold values from -0.1875 to 0.1875
- w_down: bfloat16 [256, 512, 1024], P('ep', None, 'tp'), may hold values from -0.25 to 0.25
Outputs:
- mixed: bfloat16 [8192, 1024], P('ep', 'tp')
Inputs may be any that keep to these rules, and one draw needn't show every extreme that they name: `routing`: each row names 2 different experts, all in the same group of 8 consecutive expert numbers. Among the rows of one device (aligned blocks of 64 rows) no expert is named more than 8 times, and in every block some expert is named exactly 8 times.
All inputs are finite; a program needn't handle non-finite values.
Results may differ from a plain program's by a relative error of at most 0.0015.
Values may be sent and summed in bfloat16 or wider, within the bound.
A program may use at most 64 MiB of HBM per device.

v0:
```python
import functools

import jax
import jax.numpy as jnp
from jax import lax
from jax.experimental import pallas as pl
from jax.experimental.pallas import tpu as pltpu
from jax.sharding import PartitionSpec as P

CAP = 8
EPSILON = 1e-06
MESH = pl.DeviceIdType.MESH


GROUPS = 4


def each(count, body):
    if count <= 16:
        for j in range(1, count):
            body(j)
    else:
        lax.fori_loop(1, count, lambda j, c: (body(j), c)[1], 0)


def ahead(me, j, n):
    return lax.rem(me + n - j, n)


def behind(me, j, n):
    return lax.rem(me + j, n)


def kernel(
    n, tok_hbm, gain_hbm, routing_hbm, weight_hbm, wg_hbm, wu_hbm, wd_hbm, out_ref,
    tok, routing, weight, gains, wg, wu, wd, give_g, give_u, give_d, send_x, recv_x, send_y, recv_y,
    in_sem, own_sem, give_sem, far_send, far_recv, sx_sem, rx_sem, sy_sem, ry_sem,
):
    me, core = lax.axis_index("ep"), lax.axis_index("tp")
    other = 1 - core
    tokens, half = tok.shape
    slots = 2 * n * CAP
    span = n // GROUPS

    stores = ((wg_hbm, wg, give_g), (wu_hbm, wu, give_u), (wd_hbm, wd, give_d))
    inputs = ((routing_hbm, routing), (tok_hbm, tok), (weight_hbm, weight), (gain_hbm, gains.at[core]))
    inputs = [pltpu.make_async_copy(src, dst, in_sem.at[i]) for i, (src, dst) in enumerate(inputs)]
    own = [
        pltpu.make_async_copy(src.at[core], dst.at[core], own_sem.at[i])
        for i, (src, dst, _) in enumerate(stores)
    ]
    give = [
        pltpu.make_async_copy(src.at[other], stage, give_sem.at[i])
        for i, (src, _, stage) in enumerate(stores)
    ]
    for copy in inputs:
        copy.start()

    barrier = pltpu.get_barrier_semaphore()

    def greet(j):
        peer = ahead(me, j, n)
        for c in range(2):
            pl.semaphore_signal(barrier, inc=1, device_id=(peer, c), device_id_type=MESH)

    each(n, greet)
    pl.semaphore_signal(barrier, inc=1, device_id=(me, other), device_id_type=MESH)
    for copy in give + own:
        copy.start()

    experts = 2 * n
    names = lax.broadcasted_iota(jnp.int32, (experts, tokens), 0)
    row = lax.broadcasted_iota(jnp.int32, (tokens, tokens), 0)
    col = lax.broadcasted_iota(jnp.int32, (tokens, tokens), 1)
    before = (row < col).astype(jnp.float32).astype(jnp.bfloat16)
    places = lax.broadcasted_iota(jnp.int32, (slots, tokens), 0)
    inputs[0].wait()
    picks = [routing[k:k + 1, :] for k in range(2)]
    hot = [(picks[k] == names).astype(jnp.float32) for k in range(2)]
    earlier = jnp.dot((hot[0] + hot[1]).astype(jnp.bfloat16), before, preferred_element_type=jnp.float32)
    chosen = []
    for k in range(2):
        rank = jnp.sum(earlier * hot[k], axis=0, keepdims=True).astype(jnp.int32)
        chosen.append((places == picks[k] * CAP + rank).astype(jnp.float32))
    spread = (chosen[0] + chosen[1]).astype(jnp.bfloat16)
    inputs[1].wait()
    outgoing = jnp.dot(spread, tok[...], preferred_element_type=jnp.float32)
    send_x[...] = outgoing.reshape(2 * n, CAP, half).astype(jnp.bfloat16)
    pick_rows = [jnp.transpose(c).astype(jnp.bfloat16) for c in chosen]
    inputs[2].wait()
    pick_weight = [jnp.transpose(jnp.broadcast_to(weight[k:k + 1, :], (CAP, tokens)))[:, :1] for k in range(2)]
    for copy in inputs[3:] + give:
        copy.wait()

    pl.semaphore_wait(barrier, 2 * n - 1)

    def remote(src, dst, send, recv, peer, c):
        return pltpu.make_async_remote_copy(
            src_ref=src, dst_ref=dst, send_sem=send, recv_sem=recv,
            device_id=(peer, c), device_id_type=MESH,
        )

    def block(j, h):
        return (j // span * 2 + h) * span + j % span

    gain_copy = remote(gains.at[core], gains.at[core], far_send.at[3], far_recv.at[3], me, other)
    gain_copy.start()
    remote(send_x.at[me * 2 + other], recv_x.at[block(0, core)], sx_sem, rx_sem.at[0], me, other).start()
    pltpu.make_async_copy(send_x.at[me * 2 + core], recv_x.at[block(0, core)], rx_sem.at[0]).start()

    def post(j):
        peer = ahead(me, j, n)
        for c in range(2):
            remote(
                send_x.at[peer * 2 + c], recv_x.at[block(j, core)], sx_sem, rx_sem.at[j // span], peer, c
            ).start()

    far = [
        remote(stage, dst.at[core], far_send.at[i], far_recv.at[i], me, other)
        for i, (_, dst, stage) in enumerate(stores)
    ]
    for copy in far:
        copy.start()
    each(n, post)

    for copy in own:
        copy.wait()
    gain_copy.wait()

    def reply(j):
        peer = behind(me, j, n)
        for c in range(2):
            remote(send_y.at[block(j, c)], recv_y.at[me * 2 + core], sy_sem, ry_sem, peer, c).start()

    rows = span * CAP
    for g in range(GROUPS):
        here = recv_x.at[pl.ds(2 * g * span, 2 * span)]
        pltpu.make_async_copy(here, here, rx_sem.at[g]).wait()
        parts = [
            recv_x[(2 * g + h) * span:(2 * g + h + 1) * span].astype(jnp.float32).reshape(rows, half)
            for h in range(2)
        ]
        squares = sum(jnp.sum(p * p, axis=1, keepdims=True) for p in parts)
        scale = lax.rsqrt(squares / (2 * half) + EPSILON)
        normed = jnp.concatenate(
            [(p * scale * gains[h]).astype(jnp.bfloat16) for h, p in enumerate(parts)], axis=1
        )
        if g == 0:
            far[0].wait()
            far[1].wait()
        hidden = []
        for h in range(2):
            gate = jnp.dot(normed, wg[h], preferred_element_type=jnp.float32)
            up = jnp.dot(normed, wu[h], preferred_element_type=jnp.float32)
            hidden.append((jax.nn.silu(gate) * up).astype(jnp.bfloat16))
        hidden = jnp.concatenate(hidden, axis=1)
        if g == 0:
            far[2].wait()
        for f in range(2):
            result = jnp.dot(hidden, wd[f], preferred_element_type=jnp.float32)
            first = (2 * g + f) * span
            send_y[first:first + span] = result.reshape(span, CAP, half).astype(jnp.bfloat16)
        if g == 0:
            remote(send_y.at[block(0, other)], recv_y.at[me * 2 + core], sy_sem, ry_sem, me, other).start()
            pltpu.make_async_copy(send_y.at[block(0, core)], recv_y.at[me * 2 + core], ry_sem).start()
        if span <= 16:
            for j in range(max(g * span, 1), (g + 1) * span):
                reply(j)
        else:
            lax.fori_loop(max(g * span, 1), (g + 1) * span, lambda j, c: (reply(j), c)[1], 0)

    pltpu.make_async_copy(recv_y, recv_y, ry_sem).wait()
    back = recv_y[...].astype(jnp.float32).reshape(slots, half).astype(jnp.bfloat16)
    total = 0.0
    for k in range(2):
        total = total + pick_weight[k] * jnp.dot(pick_rows[k], back, preferred_element_type=jnp.float32)
    out_ref[...] = total.astype(jnp.bfloat16)
    sent = pl.ds(0, 2 * n - 1)
    pltpu.make_async_copy(send_x.at[sent], send_x.at[sent], sx_sem).wait()
    pltpu.make_async_copy(send_y.at[sent], send_y.at[sent], sy_sem).wait()


def solution(mesh):
    n = mesh.shape["ep"]

    def local(tokens, norm_gain, routing, route_weight, w_gate, w_up, w_down):
        rows, half = tokens.shape
        assert w_gate.shape[0] == 2 and mesh.shape["tp"] == 2
        vmem = pl.BlockSpec(memory_space=pltpu.VMEM)
        far = pl.BlockSpec(memory_space=pl.ANY)
        blocks = pltpu.VMEM((2 * n, CAP, half), jnp.bfloat16)
        dma = pltpu.SemaphoreType.DMA
        return pl.pallas_call(
            functools.partial(kernel, n),
            out_shape=pltpu.VMEM((rows, half), jnp.bfloat16),
            in_specs=[far] * 7,
            out_specs=vmem,
            scratch_shapes=[
                pltpu.VMEM((rows, half), jnp.bfloat16),
                pltpu.VMEM((2, rows), jnp.int32),
                pltpu.VMEM((2, rows), jnp.float32),
                pltpu.VMEM((2, 1, half), jnp.float32),
                pltpu.VMEM(w_gate.shape, jnp.bfloat16),
                pltpu.VMEM(w_up.shape, jnp.bfloat16),
                pltpu.VMEM(w_down.shape, jnp.bfloat16),
                pltpu.VMEM(w_gate.shape[1:], jnp.bfloat16),
                pltpu.VMEM(w_up.shape[1:], jnp.bfloat16),
                pltpu.VMEM(w_down.shape[1:], jnp.bfloat16),
                blocks, blocks, blocks, blocks,
                dma((4,)), dma((3,)), dma((3,)), dma((4,)), dma((4,)), dma, dma((GROUPS,)), dma, dma,
            ],
            compiler_params=pltpu.CompilerParams(collective_id=0, has_side_effects=True),
            name="experts",
        )(tokens, norm_gain.reshape(1, half), routing.T, route_weight.T, w_gate, w_up, w_down)

    in_specs = (
        P("ep", "tp"), P("tp"), P("ep", None), P("ep", None),
        P("ep", None, "tp"), P("ep", None, "tp"), P("ep", None, "tp"),
    )
    return jax.shard_map(local, mesh=mesh, in_specs=in_specs, out_specs=P("ep", "tp"), check_vma=False)
```

profile of v0, /device:TPU:63, one launch (start us, length us, event | category | flops | bytes accessed | tf_op | source)
XLA Modules:
  0.0 129.9 jit_solution(10104654534880316955)
XLA Ops:
  0.0 129.2 %experts.1 = bf16[64,512]{1,0:T(8,128)(2,1)S(1)} custom-call(bf16[64,512]{1,0:T(8,128)(2,1)} %tok_hbm.1, f32[1,512]{1,0:T(1,128)} %bitcast.3, s32[2,64]{1,0:T(2,128)} %bitcast.4, f32[2,64]{1,0:T(2,128)} %bitcast.5, bf16[2,1024,256]{2,1,0:T(8,128)(2,1)} %wg_hbm.1, bf16[2,1024,256]{2,1,0:T(8,128)(2,1)} %wu_hbm.1, bf16[2,512,512]{2,1,0:T(8,128)(2,1)} %wd_hbm.1), custom_call_target="tpu_custom_call" | custom-call | tf_op jit(solution)/shard_map/experts/pallas_call | solution.py:193
  129.2 0.6 copy.9
where the time goes:
time: 130 us
  Pallas kernels  129 us (99%)
    pallas_call x1, Pallas kernels, local(): pl.pallas_call(functools.partial(kernel, n), out_shape=pltpu.VMEM((rows,...  129 us

commit v1 on v0

v1 whole, which is shorter than its diff:
```python
import functools

import jax
import jax.numpy as jnp
from jax import lax
from jax.experimental import pallas as pl
from jax.experimental.pallas import tpu as pltpu
from jax.sharding import PartitionSpec as P

CAP = 8
EPSILON = 1e-06
MESH = pl.DeviceIdType.MESH

Z, Y, X = 8, 4, 4
EXPERTS = 2 * X
SLOTS = EXPERTS * CAP // 2
OFFSETS = Z * Y
STEPS = (0, 1, 7, 2, 6, 3, 5, 4)
ROUNDS = ((0, 1), (1, 3), (3, 5), (5, 7), (7, 8))
SEND_ORDER = (0, 1, 2, 3, 4)
ORDER = (
    "A0", "A1", "F0", "A2", "F1", "C0", "A3", "F2", "C1", "A4", "F3", "C2", "F4", "C3", "C4",
    "H0", "H1", "H2", "H3", "H4",
)


def kernel(
    tok_hbm, gain_hbm, routing_hbm, weight_hbm, wg_hbm, wu_hbm, wd_hbm, out_ref,
    tok, routing, weight, gains, wg, wu, wd, give_g, give_u, give_d,
    meta_s, meta_r, pick_home, send_1, recv_1, send_2, recv_2, send_3, recv_3, send_4, recv_4,
    in_sem, own_sem, give_sem, far_send, far_recv, s_sem, meta_sem, sem_1, sem_2, sem_3, sem_4,
):
    me, core = lax.axis_index("ep"), lax.axis_index("tp")
    other = 1 - core
    z, y, x = me // (Y * X), me // X % Y, me % X
    tokens, half = tok.shape

    def plane(step, dy, sign):
        if sign > 0:
            return ((z + step) % Z * Y + (y + dy) % Y) * X + x
        return ((z + Z - step) % Z * Y + (y + Y - dy) % Y) * X + x

    def line(dx, sign):
        return me - x + (x + (dx if sign > 0 else X - dx)) % X

    stores = ((wg_hbm, wg, give_g), (wu_hbm, wu, give_u), (wd_hbm, wd, give_d))
    inputs = ((routing_hbm, routing), (weight_hbm, weight), (tok_hbm, tok), (gain_hbm, gains.at[core]))
    inputs = [pltpu.make_async_copy(src, dst, in_sem.at[i]) for i, (src, dst) in enumerate(inputs)]
    own = [
        pltpu.make_async_copy(src.at[core], dst.at[core], own_sem.at[i])
        for i, (src, dst, _) in enumerate(stores)
    ]
    give = [
        pltpu.make_async_copy(src.at[other], stage, give_sem.at[i])
        for i, (src, _, stage) in enumerate(stores)
    ]
    for copy in inputs:
        copy.start()

    barrier = pltpu.get_barrier_semaphore()
    greeted = 0
    for step in STEPS:
        for dy in range(Y):
            if step or dy:
                pl.semaphore_signal(barrier, inc=1, device_id=(plane(step, dy, 1), core), device_id_type=MESH)
                greeted += 1
    for dx in range(X):
        for c in range(2):
            if dx:
                pl.semaphore_signal(barrier, inc=1, device_id=(line(dx, 1), c), device_id_type=MESH)
                greeted += 1
    pl.semaphore_signal(barrier, inc=1, device_id=(me, other), device_id_type=MESH)
    greeted += 1
    for copy in give + own:
        copy.start()

    row = lax.broadcasted_iota(jnp.int32, (tokens, tokens), 0)
    col = lax.broadcasted_iota(jnp.int32, (tokens, tokens), 1)
    before = (row < col).astype(jnp.float32).astype(jnp.bfloat16)
    names = lax.broadcasted_iota(jnp.int32, (OFFSETS * EXPERTS, tokens), 0)
    inputs[0].wait()
    picks = [routing[k:k + 1, :] for k in range(2)]
    group = picks[0] // EXPERTS
    dz = (group // Y - z + Z) % Z
    dy = (group % Y - y + Y) % Y
    place = jnp.where(dz <= Z // 2, jnp.maximum(2 * dz - 1, 0), 2 * (Z - dz)) * Y + dy
    hot = [(picks[k] == names).astype(jnp.float32) for k in range(2)]
    hot_place = (place == names[:OFFSETS]).astype(jnp.float32)
    both = jnp.concatenate([hot[0] + hot[1], hot_place], axis=0).astype(jnp.bfloat16)
    earlier = jnp.dot(both, before, preferred_element_type=jnp.float32)
    slot = jnp.sum(earlier[OFFSETS * EXPERTS:] * hot_place, axis=0, keepdims=True)
    spot = place.astype(jnp.float32) * SLOTS + slot
    codes = [
        (picks[k] % EXPERTS * CAP + 1).astype(jnp.float32)
        + jnp.sum(earlier[:OFFSETS * EXPERTS] * hot[k], axis=0, keepdims=True)
        for k in range(2)
    ]
    inputs[1].wait()
    rows = [spot] + codes + [weight[k:k + 1, :] for k in range(2)] + [jnp.zeros_like(spot)] * 3
    columns = jnp.transpose(jnp.concatenate(rows, axis=0))
    slots = OFFSETS * SLOTS
    lanes = lax.broadcasted_iota(jnp.int32, (tokens, slots), 1)
    at_home = lanes == columns[:, 0:1].astype(jnp.int32)
    pick_home[...] = at_home.astype(jnp.float32).astype(jnp.bfloat16)
    for q in range(4):
        values = jnp.sum(jnp.where(at_home, columns[:, q + 1:q + 2], 0.0), axis=0, keepdims=True)
        for p in range(Z):
            meta_s[p, q:q + 1, :] = values[:, p * Y * SLOTS:(p + 1) * Y * SLOTS]
    spread = lax.broadcasted_iota(jnp.int32, (slots, tokens), 0) == spot.astype(jnp.int32)
    spread = spread.astype(jnp.float32).astype(jnp.bfloat16)
    inputs[2].wait()
    outgoing = jnp.dot(spread, tok[...], preferred_element_type=jnp.float32)
    send_1[...] = outgoing.astype(jnp.bfloat16).reshape(OFFSETS, SLOTS, half)
    inputs[3].wait()

    pl.semaphore_wait(barrier, greeted)

    def remote(src, dst, send, recv, peer, c):
        return pltpu.make_async_remote_copy(
            src_ref=src, dst_ref=dst, send_sem=send, recv_sem=recv,
            device_id=(peer, c), device_id_type=MESH,
        )

    pltpu.make_async_copy(meta_s.at[0], meta_r.at[0], meta_sem.at[0]).start()
    pltpu.make_async_copy(send_1.at[0], recv_1.at[0], sem_1.at[0]).start()
    for r in SEND_ORDER:
        for dy in range(Y):
            for p in range(*ROUNDS[r]):
                if p or dy:
                    o, peer = p * Y + dy, plane(STEPS[p], dy, 1)
                    remote(meta_s.at[p], meta_r.at[o], s_sem.at[0], meta_sem.at[r], peer, core).start()
                    remote(send_1.at[o], recv_1.at[o], s_sem.at[1], sem_1.at[r], peer, core).start()

    gain_copy = remote(gains.at[core], gains.at[core], far_send.at[3], far_recv.at[3], me, other)
    gain_copy.start()
    for copy in give:
        copy.wait()
    far = [
        remote(stage, dst.at[core], far_send.at[i], far_recv.at[i], me, other)
        for i, (_, dst, stage) in enumerate(stores)
    ]
    for copy in far:
        copy.start()

    def arrived(ref, sem):
        pltpu.make_async_copy(ref, ref, sem).wait()

    def codes_of(r):
        parts = []
        segment = lax.broadcasted_iota(jnp.int32, (4, Y * SLOTS), 1) // SLOTS
        for p in range(*ROUNDS[r]):
            part = jnp.zeros((4, Y * SLOTS), jnp.float32)
            for dy in range(Y):
                part = jnp.where(segment == dy, meta_r[p * Y + dy], part)
            parts.append(part)
        return parts

    def full(code, block, blocks):
        code = code.astype(jnp.int32) - 1
        return (code >> 3) * (blocks * CAP) + block * CAP + (code & 7)

    def extent(r):
        first, last = ROUNDS[r]
        return first * Y, (last - first) * Y

    def step_a(r):
        first, blocks = extent(r)
        here = pl.ds(first, blocks)
        arrived(meta_r.at[here], meta_sem.at[r])
        table = codes_of(r)
        table = jnp.concatenate(table, axis=1) if len(table) > 1 else table[0]
        block = lax.broadcasted_iota(jnp.int32, (1, blocks * SLOTS), 1) // SLOTS
        places = lax.broadcasted_iota(jnp.int32, (EXPERTS * blocks * CAP, blocks * SLOTS), 0)
        hit = [places == full(table[k:k + 1, :], block, blocks) for k in range(2)]
        pick = (hit[0] | hit[1]).astype(jnp.float32).astype(jnp.bfloat16)
        arrived(recv_1.at[here], sem_1.at[r])
        source = recv_1[first:first + blocks].reshape(blocks * SLOTS, half)
        lined = jnp.dot(pick, source, preferred_element_type=jnp.float32).astype(jnp.bfloat16)
        at = pl.ds(first * CAP, blocks * CAP)
        send_2[:, first * CAP:(first + blocks) * CAP, :] = lined.reshape(EXPERTS, blocks * CAP, half)
        for dx in (2, 1, 3):
            peer = line(dx, 1)
            for c in range(2):
                remote(
                    send_2.at[(x + dx) % X * 2 + c, at], recv_2.at[dx, core, at], s_sem.at[2], sem_2.at[r], peer, c
                ).start()
        remote(send_2.at[x * 2 + other, at], recv_2.at[0, core, at], s_sem.at[2], sem_2.at[r], me, other).start()
        pltpu.make_async_copy(send_2.at[x * 2 + core, at], recv_2.at[0, core, at], sem_2.at[r]).start()

    ready = []

    def step_f(r):
        first, blocks = extent(r)
        count = blocks * CAP
        at = pl.ds(first * CAP, count)
        arrived(recv_2.at[:, :, at], sem_2.at[r])
        if not ready:
            gain_copy.wait()
        parts = [
            recv_2[:, h, first * CAP:first * CAP + count, :].astype(jnp.float32).reshape(X * count, half)
            for h in range(2)
        ]
        squares = sum(jnp.sum(p * p, axis=1, keepdims=True) for p in parts)
        scale = lax.rsqrt(squares / (2 * half) + EPSILON)
        normed = jnp.concatenate(
            [(p * scale * gains[h]).astype(jnp.bfloat16) for h, p in enumerate(parts)], axis=1
        )
        if not ready:
            for copy in own + far[:2]:
                copy.wait()
        hidden = []
        for h in range(2):
            gate = jnp.dot(normed, wg[h], preferred_element_type=jnp.float32)
            up = jnp.dot(normed, wu[h], preferred_element_type=jnp.float32)
            hidden.append((jax.nn.silu(gate) * up).astype(jnp.bfloat16))
        hidden = jnp.concatenate(hidden, axis=1)
        if not ready:
            far[2].wait()
            ready.append(True)
        for f in range(2):
            result = jnp.dot(hidden, wd[f], preferred_element_type=jnp.float32).astype(jnp.bfloat16)
            send_3[:, f, first * CAP:first * CAP + count, :] = result.reshape(X, count, half)
        mine = x * 2 + core
        for dx in (2, 1, 3):
            peer = line(dx, -1)
            for c in range(2):
                remote(
                    send_3.at[dx, c, at], recv_3.at[mine, at], s_sem.at[3], sem_3.at[r], peer, c
                ).start()
        remote(send_3.at[0, other, at], recv_3.at[mine, at], s_sem.at[3], sem_3.at[r], me, other).start()
        pltpu.make_async_copy(send_3.at[0, core, at], recv_3.at[mine, at], sem_3.at[r]).start()

    def step_c(r):
        first, blocks = extent(r)
        at = pl.ds(first * CAP, blocks * CAP)
        table = [jnp.transpose(jnp.concatenate([t, jnp.zeros_like(t)], axis=0)) for t in codes_of(r)]
        table = jnp.concatenate(table, axis=0) if len(table) > 1 else table[0]
        block = lax.broadcasted_iota(jnp.int32, (blocks * SLOTS, 1), 0) // SLOTS
        places = lax.broadcasted_iota(jnp.int32, (blocks * SLOTS, EXPERTS * blocks * CAP), 1)
        take = [
            (places == full(table[:, k:k + 1], block, blocks)).astype(jnp.float32).astype(jnp.bfloat16)
            for k in range(2)
        ]
        arrived(recv_3.at[:, at], sem_3.at[r])
        source = recv_3[:, first * CAP:(first + blocks) * CAP, :].reshape(EXPERTS * blocks * CAP, half)
        total = 0.0
        for k in range(2):
            total = total + table[:, 2 + k:3 + k] * jnp.dot(take[k], source, preferred_element_type=jnp.float32)
        send_4[first:first + blocks] = total.astype(jnp.bfloat16).reshape(blocks, SLOTS, half)
        for dy in range(Y):
            for p in range(*ROUNDS[r]):
                o = p * Y + dy
                if o:
                    remote(
                        send_4.at[o], recv_4.at[o], s_sem.at[4], sem_4.at[r], plane(STEPS[p], dy, -1), core
                    ).start()
                else:
                    pltpu.make_async_copy(send_4.at[0], recv_4.at[0], sem_4.at[r]).start()

    sums = []

    def step_h(r):
        first, blocks = extent(r)
        here = pl.ds(first, blocks)
        arrived(recv_4.at[here], sem_4.at[r])
        source = recv_4[first:first + blocks].reshape(blocks * SLOTS, half)
        take = pick_home[:, first * SLOTS:(first + blocks) * SLOTS]
        sums.append(jnp.dot(take, source, preferred_element_type=jnp.float32))

    step_of = {"A": step_a, "F": step_f, "C": step_c, "H": step_h}
    for name in ORDER:
        step_of[name[0]](int(name[1]))
    out_ref[...] = sum(sums).astype(jnp.bfloat16)

    arrived(meta_r.at[pl.ds(1, OFFSETS - 1)], s_sem.at[0])
    arrived(send_1.at[pl.ds(1, OFFSETS - 1)], s_sem.at[1])
    arrived(send_2.at[pl.ds(1, EXPERTS - 1)], s_sem.at[2])
    arrived(send_2.at[pl.ds(1, EXPERTS - 1)], s_sem.at[3])
    arrived(send_4.at[pl.ds(1, OFFSETS - 1)], s_sem.at[4])


def solution(mesh):
    assert mesh.shape["ep"] == Z * Y * X and mesh.shape["tp"] == 2

    def local(tokens, norm_gain, routing, route_weight, w_gate, w_up, w_down):
        rows, half = tokens.shape
        vmem = pl.BlockSpec(memory_space=pltpu.VMEM)
        far = pl.BlockSpec(memory_space=pl.ANY)
        dma = pltpu.SemaphoreType.DMA
        bf16, f32 = jnp.bfloat16, jnp.float32
        blocks = OFFSETS * CAP
        rounds = dma((len(ROUNDS),))
        return pl.pallas_call(
            kernel,
            out_shape=pltpu.VMEM((rows, half), bf16),
            in_specs=[far] * 7,
            out_specs=vmem,
            scratch_shapes=[
                pltpu.VMEM((rows, half), bf16),
                pltpu.VMEM((2, rows), jnp.int32),
                pltpu.VMEM((2, rows), f32),
                pltpu.VMEM((2, 1, half), f32),
                pltpu.VMEM(w_gate.shape, bf16),
                pltpu.VMEM(w_up.shape, bf16),
                pltpu.VMEM(w_down.shape, bf16),
                pltpu.VMEM(w_gate.shape[1:], bf16),
                pltpu.VMEM(w_up.shape[1:], bf16),
                pltpu.VMEM(w_down.shape[1:], bf16),
                pltpu.VMEM((Z, 4, Y * SLOTS), f32),
                pltpu.VMEM((OFFSETS, 4, Y * SLOTS), f32),
                pltpu.VMEM((rows, OFFSETS * SLOTS), bf16),
                pltpu.VMEM((OFFSETS, SLOTS, half), bf16),
                pltpu.VMEM((OFFSETS, SLOTS, half), bf16),
                pltpu.VMEM((EXPERTS, blocks, half), bf16),
                pltpu.VMEM((X, 2, blocks, half), bf16),
                pltpu.VMEM((X, 2, blocks, half), bf16),
                pltpu.VMEM((EXPERTS, blocks, half), bf16),
                pltpu.VMEM((OFFSETS, SLOTS, half), bf16),
                pltpu.VMEM((OFFSETS, SLOTS, half), bf16),
                dma((4,)), dma((3,)), dma((3,)), dma((4,)), dma((4,)), dma((5,)),
                rounds, rounds, rounds, rounds, rounds,
            ],
            compiler_params=pltpu.CompilerParams(collective_id=0, has_side_effects=True),
            name="experts",
        )(tokens, norm_gain.reshape(1, half), routing.T, route_weight.T, w_gate, w_up, w_down)

    in_specs = (
        P("ep", "tp"), P("tp"), P("ep", None), P("ep", None),
        P("ep", None, "tp"), P("ep", None, "tp"), P("ep", None, "tp"),
    )
    return jax.shard_map(local, mesh=mesh, in_specs=in_specs, out_specs=P("ep", "tp"), check_vma=False)
```

time: 130 us -> 84.5 us (0.65)
  the two profiles are of different devices: /device:TPU:63 before, /device:TPU:1 now
where the time goes in v1:
time: 84.5 us; the launch traced here: 84.4 us
  Pallas kernels  83.8 us (99%)
    pallas_call x1, Pallas kernels, local(): pl.pallas_call(kernel, out_shape=pltpu.VMEM((rows, half), bf16), in_specs...  83.8 us

profile of v1, /device:TPU:1, one launch (start us, length us, event | category | flops | bytes accessed | tf_op | source)
XLA Modules:
  0.0 84.4 jit_solution(13216421962180493643)
XLA Ops:
  0.0 83.8 %experts.1 = bf16[64,512]{1,0:T(8,128)(2,1)S(1)} custom-call(bf16[64,512]{1,0:T(8,128)(2,1)} %tok_hbm.1, f32[1,512]{1,0:T(1,128)} %bitcast.3, s32[2,64]{1,0:T(2,128)} %bitcast.4, f32[2,64]{1,0:T(2,128)} %bitcast.5, bf16[2,1024,256]{2,1,0:T(8,128)(2,1)} %wg_hbm.1, bf16[2,1024,256]{2,1,0:T(8,128)(2,1)} %wu_hbm.1, bf16[2,512,512]{2,1,0:T(8,128)(2,1)} %wd_hbm.1), custom_call_target="tpu_custom_call" | custom-call | tf_op jit(solution)/shard_map/experts/pallas_call | solution.py:293
  83.8 0.6 copy.9

commit v2 on v1

--- a/solution.py
+++ b/solution.py
@@ -16,11 +16,11 @@
 SLOTS = EXPERTS * CAP // 2
 OFFSETS = Z * Y
 STEPS = (0, 1, 7, 2, 6, 3, 5, 4)
-ROUNDS = ((0, 1), (1, 3), (3, 5), (5, 7), (7, 8))
-SEND_ORDER = (0, 1, 2, 3, 4)
+ROUNDS = tuple((p, p + 1) for p in range(Z))
+SEND_ORDER = (0, 1, 4, 6, 5, 3, 2, 7)
 ORDER = (
-    "A0", "A1", "F0", "A2", "F1", "C0", "A3", "F2", "C1", "A4", "F3", "C2", "F4", "C3", "C4",
-    "H0", "H1", "H2", "H3", "H4",
+    "A0", "A1", "A4", "F1", "F4", "A5", "A6", "F5", "C4", "A7", "C1", "F6", "A3", "C5", "F7", "A2",
+    "C6", "F3", "C7", "F2", "F0", "C3", "C2", "C0", "H4", "H1", "H5", "H6", "H7", "H3", "H2", "H0",
 )
 
 

time: 84.5 us -> 74 us (0.88)
  Pallas kernels: 83.8 us -> 73.3 us
    pallas_call x1, Pallas kernels: 83.8 us -> 73.3 us  [local(): pl.pallas_call(kernel, out_shape=pltpu.VMEM((rows, half), bf16), in_specs...]
where the time goes in v2:
time: 74 us; the launch traced here: 73.9 us
  Pallas kernels  73.3 us (99%)
    pallas_call x1, Pallas kernels, local(): pl.pallas_call(kernel, out_shape=pltpu.VMEM((rows, half), bf16), in_specs...  73.3 us

profile of v2, /device:TPU:1, one launch (start us, length us, event | category | flops | bytes accessed | tf_op | source)
XLA Modules:
  0.0 73.9 jit_solution(3888829916156938581)
XLA Ops:
  0.0 73.3 %experts.1 = bf16[64,512]{1,0:T(8,128)(2,1)S(1)} custom-call(bf16[64,512]{1,0:T(8,128)(2,1)} %tok_hbm.1, f32[1,512]{1,0:T(1,128)} %bitcast.3, s32[2,64]{1,0:T(2,128)} %bitcast.4, f32[2,64]{1,0:T(2,128)} %bitcast.5, bf16[2,1024,256]{2,1,0:T(8,128)(2,1)} %wg_hbm.1, bf16[2,1024,256]{2,1,0:T(8,128)(2,1)} %wu_hbm.1, bf16[2,512,512]{2,1,0:T(8,128)(2,1)} %wd_hbm.1), custom_call_target="tpu_custom_call" | custom-call | tf_op jit(solution)/shard_map/experts/pallas_call | solution.py:293
  73.3 0.6 copy.9

commit v3 on v2

v3 whole, which is shorter than its diff:
```python
import functools

import jax
import jax.numpy as jnp
from jax import lax
from jax.experimental import pallas as pl
from jax.experimental.pallas import tpu as pltpu
from jax.sharding import PartitionSpec as P

CAP = 8
EPSILON = 1e-06
MESH = pl.DeviceIdType.MESH

Z, Y, X = 8, 4, 4
EXPERTS = 2 * X
SLOTS = EXPERTS * CAP // 2
OFFSETS = Z * Y
STEPS = (0, 1, 7, 2, 6, 3, 5, 4)
LINE = (2, 1, 3)
COLUMN = (2, 1, 3)
ORDER = """
    G00 G01 G03 G02 A0 G10 G11 G13 G12 A1 A2 G20 G21 F0 G23 G22 A3 A4 F1 G30 G31 C0 G33 G32 A5 A6 F2 F3 C1
    A7 F4 C2 E0 F5 E1 C3 F6 E2 C4 F7 C5 E3 C6 E4 C7 E5 E6 E7 H0 H1 H2 H3 H4 H5 H6 H7
"""


def kernel(
    tok_hbm, gain_hbm, routing_hbm, weight_hbm, wg_hbm, wu_hbm, wd_hbm, out_ref,
    routing, weight, gains, wg, wu, wd, give_g, give_u, give_d,
    meta_s, meta_r, blocks, tables, send_2, recv_2, send_3, recv_3, send_4, recv_4, send_5, recv_5,
    in_sem, own_sem, give_sem, far_send, far_recv, s_sem, meta_sem, block_sem, table_sem, sem_2, sem_3, sem_4, sem_5,
):
    me, core = lax.axis_index("ep"), lax.axis_index("tp")
    other = 1 - core
    z, y, x = me // (Y * X), me // X % Y, me % X
    tokens, half = blocks.shape[2:]
    place_of = {step: p for p, step in enumerate(STEPS)}

    def plane(step, dy, sign):
        if sign > 0:
            return ((z + step) % Z * Y + (y + dy) % Y) * X + x
        return ((z + Z - step) % Z * Y + (y + Y - dy) % Y) * X + x

    def line(dx, sign):
        return me - x + (x + (dx if sign > 0 else X - dx)) % X

    stores = ((wg_hbm, wg, give_g), (wu_hbm, wu, give_u), (wd_hbm, wd, give_d))
    inputs = ((routing_hbm, routing), (weight_hbm, weight), (tok_hbm, blocks.at[0, 0]), (gain_hbm, gains.at[core]))
    inputs = [pltpu.make_async_copy(src, dst, in_sem.at[i]) for i, (src, dst) in enumerate(inputs)]
    own = [
        pltpu.make_async_copy(src.at[core], dst.at[core], own_sem.at[i])
        for i, (src, dst, _) in enumerate(stores)
    ]
    give = [
        pltpu.make_async_copy(src.at[other], stage, give_sem.at[i])
        for i, (src, _, stage) in enumerate(stores)
    ]
    for copy in inputs:
        copy.start()

    barrier = pltpu.get_barrier_semaphore()
    greeted = 0
    for step in STEPS:
        for dy in range(Y):
            if step or dy:
                pl.semaphore_signal(barrier, inc=1, device_id=(plane(step, dy, 1), core), device_id_type=MESH)
                greeted += 1
    for dy in range(1, Y):
        pl.semaphore_signal(barrier, inc=1, device_id=(plane(0, dy, 1), other), device_id_type=MESH)
        greeted += 1
    for dx in range(X):
        for c in range(2):
            if dx:
                pl.semaphore_signal(barrier, inc=1, device_id=(line(dx, 1), c), device_id_type=MESH)
                greeted += 1
    pl.semaphore_signal(barrier, inc=1, device_id=(me, other), device_id_type=MESH)
    greeted += 1
    for copy in give + own:
        copy.start()

    row = lax.broadcasted_iota(jnp.int32, (tokens, tokens), 0)
    col = lax.broadcasted_iota(jnp.int32, (tokens, tokens), 1)
    before = (row < col).astype(jnp.float32).astype(jnp.bfloat16)
    names = lax.broadcasted_iota(jnp.int32, (OFFSETS * EXPERTS, tokens), 0)
    inputs[0].wait()
    picks = [routing[k:k + 1, :] for k in range(2)]
    group = picks[0] // EXPERTS
    dz = (group // Y - z + Z) % Z
    dy = (group % Y - y + Y) % Y
    place = jnp.where(dz <= Z // 2, jnp.maximum(2 * dz - 1, 0), 2 * (Z - dz)) * Y + dy
    hot = [(picks[k] == names).astype(jnp.float32) for k in range(2)]
    hot_place = (place == names[:OFFSETS]).astype(jnp.float32)
    both = jnp.concatenate([hot[0] + hot[1], hot_place], axis=0).astype(jnp.bfloat16)
    earlier = jnp.dot(both, before, preferred_element_type=jnp.float32)
    slot = jnp.sum(earlier[OFFSETS * EXPERTS:] * hot_place, axis=0, keepdims=True)
    spot = place.astype(jnp.float32) * SLOTS + slot
    ranks = [jnp.sum(earlier[:OFFSETS * EXPERTS] * hot[k], axis=0, keepdims=True) for k in range(2)]
    codes = [(picks[k] % EXPERTS * CAP + 1).astype(jnp.float32) + ranks[k] for k in range(2)]
    seats = [(picks[k] * CAP).astype(jnp.float32) + ranks[k] for k in range(2)]
    inputs[1].wait()
    rows = [spot] + codes + [weight[k:k + 1, :] for k in range(2)] + seats + [spot]
    columns = jnp.transpose(jnp.concatenate(rows, axis=0))
    slots = OFFSETS * SLOTS
    lanes = lax.broadcasted_iota(jnp.int32, (tokens, slots), 1)
    at_home = lanes == columns[:, 0:1].astype(jnp.int32)
    for q in range(4):
        values = jnp.sum(jnp.where(at_home, columns[:, q + 1:q + 2], 0.0), axis=0, keepdims=True)
        for p in range(Z):
            meta_s[p, q:q + 1, :] = values[:, p * Y * SLOTS:(p + 1) * Y * SLOTS]
    repeated = lax.broadcasted_iota(jnp.int32, (tokens, X * tokens), 1) % tokens
    repeated = repeated == lax.broadcasted_iota(jnp.int32, (tokens, X * tokens), 0)
    for k in range(3):
        values = jnp.where(repeated, columns[:, 5 + k:6 + k], 0.0)
        tables[0, 0, k:k + 1, :] = jnp.sum(values, axis=0, keepdims=True)
    tables[0, 0, 3:4, :] = jnp.zeros((1, X * tokens), jnp.float32)
    inputs[2].wait()
    inputs[3].wait()

    pl.semaphore_wait(barrier, greeted)

    def remote(src, dst, send, recv, peer, c):
        return pltpu.make_async_remote_copy(
            src_ref=src, dst_ref=dst, send_sem=send, recv_sem=recv,
            device_id=(peer, c), device_id_type=MESH,
        )

    def arrived(ref, sem):
        pltpu.make_async_copy(ref, ref, sem).wait()

    def pass_on(p, j, q, i, peer):
        remote(tables.at[p, j], tables.at[q, i], s_sem.at[0], table_sem.at[q, i], peer, core).start()
        remote(blocks.at[p, j], blocks.at[q, i], s_sem.at[1], block_sem.at[q, i], peer, core).start()

    up, down = plane(1, 0, 1), plane(1, 0, -1)
    middle = Z // 2

    def step_g(k, j):
        for p in sorted({place_of[k], place_of[(Z - k) % Z]}):
            chunk_here(p, j)
        if k + 1 < middle or j < X // 2:
            pass_on(place_of[k], j, place_of[k + 1], j, up)
        if k + 1 < middle or j >= X // 2:
            pass_on(place_of[(Z - k) % Z], j, place_of[Z - k - 1], j, down)

    seen = {(0, 0)}

    def chunk_here(p, j):
        if (p, j) not in seen:
            seen.add((p, j))
            arrived(tables.at[p, j], table_sem.at[p, j])
            arrived(blocks.at[p, j], block_sem.at[p, j])

    for dx in LINE:
        pass_on(0, 0, 0, dx, line(dx, 1))
    step_g(0, 0)
    pltpu.make_async_copy(meta_s.at[0], meta_r.at[0], meta_sem.at[0]).start()
    for p, step in enumerate(STEPS):
        for dy in range(Y):
            if p or dy:
                o, peer = p * Y + dy, plane(step, dy, 1)
                remote(meta_s.at[p], meta_r.at[o], s_sem.at[2], meta_sem.at[p], peer, core).start()

    gain_copy = remote(gains.at[core], gains.at[core], far_send.at[3], far_recv.at[3], me, other)
    gain_copy.start()
    for copy in give:
        copy.wait()
    far = [
        remote(stage, dst.at[core], far_send.at[i], far_recv.at[i], me, other)
        for i, (_, dst, stage) in enumerate(stores)
    ]
    for copy in far:
        copy.start()

    def codes_of(p):
        segment = lax.broadcasted_iota(jnp.int32, (4, Y * SLOTS), 1) // SLOTS
        table = jnp.zeros((4, Y * SLOTS), jnp.float32)
        for dy in range(Y):
            table = jnp.where(segment == dy, meta_r[p * Y + dy], table)
        return table

    def step_a(p):
        for j in range(X):
            chunk_here(p, j)
        spot_of = lax.broadcasted_iota(jnp.int32, (4, X * tokens), 1) // tokens
        seat = jnp.zeros((4, X * tokens), jnp.float32)
        for j in range(X):
            seat = jnp.where(spot_of == j, tables[p, j], seat)
        seat = seat.astype(jnp.int32)
        pick = seat // CAP
        group, expert = pick // EXPERTS, pick % EXPERTS
        dy = (group % Y - y + Y) % Y
        target = ((dy * 2 + expert % 2) * X + spot_of) * CAP + seat % CAP
        target = jnp.where((group // Y == z) & (expert // 2 == x), target, -1)
        places = lax.broadcasted_iota(jnp.int32, (Y * 2 * X * CAP, X * tokens), 0)
        take = (places == target[0:1]) | (places == target[1:2])
        take = take.astype(jnp.float32).astype(jnp.bfloat16)
        source = blocks[p].reshape(X * tokens, half)
        chosen = jnp.dot(take, source, preferred_element_type=jnp.float32)
        send_2[p] = chosen.reshape(Y, 2, X, CAP, half).astype(jnp.bfloat16)
        for dy in COLUMN:
            for c in range(2):
                remote(
                    send_2.at[p, dy, c], recv_2.at[core, p, :, dy], s_sem.at[3], sem_2.at[p], plane(0, dy, 1), c
                ).start()
        remote(send_2.at[p, 0, other], recv_2.at[core, p, :, 0], s_sem.at[3], sem_2.at[p], me, other).start()
        pltpu.make_async_copy(send_2.at[p, 0, core], recv_2.at[core, p, :, 0], sem_2.at[p]).start()

    ready = []

    def step_f(p):
        count = Y * CAP
        at = pl.ds(p * count, count)
        arrived(recv_2.at[:, p], sem_2.at[p])
        if not ready:
            gain_copy.wait()
        parts = [recv_2[h, p].astype(jnp.float32).reshape(X * count, half) for h in range(2)]
        squares = sum(jnp.sum(part * part, axis=1, keepdims=True) for part in parts)
        scale = lax.rsqrt(squares / (2 * half) + EPSILON)
        normed = jnp.concatenate(
            [(part * scale * gains[h]).astype(jnp.bfloat16) for h, part in enumerate(parts)], axis=1
        )
        if not ready:
            for copy in own + far[:2]:
                copy.wait()
        hidden = []
        for h in range(2):
            gate = jnp.dot(normed, wg[h], preferred_element_type=jnp.float32)
            up = jnp.dot(normed, wu[h], preferred_element_type=jnp.float32)
            hidden.append((jax.nn.silu(gate) * up).astype(jnp.bfloat16))
        hidden = jnp.concatenate(hidden, axis=1)
        if not ready:
            far[2].wait()
            ready.append(True)
        for f in range(2):
            result = jnp.dot(hidden, wd[f], preferred_element_type=jnp.float32).astype(jnp.bfloat16)
            send_3[:, f, p * count:(p + 1) * count, :] = result.reshape(X, count, half)
        mine = x * 2 + core
        for dx in LINE:
            peer = line(dx, -1)
            for c in range(2):
                remote(
                    send_3.at[dx, c, at], recv_3.at[mine, at], s_sem.at[4], sem_3.at[p], peer, c
                ).start()
        remote(send_3.at[0, other, at], recv_3.at[mine, at], s_sem.at[4], sem_3.at[p], me, other).start()
        pltpu.make_async_copy(send_3.at[0, core, at], recv_3.at[mine, at], sem_3.at[p]).start()

    def step_c(p):
        arrived(meta_r.at[pl.ds(p * Y, Y)], meta_sem.at[p])
        table = codes_of(p)
        table = jnp.transpose(jnp.concatenate([table, jnp.zeros_like(table)], axis=0))
        block = lax.broadcasted_iota(jnp.int32, (Y * SLOTS, 1), 0) // SLOTS
        places = lax.broadcasted_iota(jnp.int32, (Y * SLOTS, EXPERTS * Y * CAP), 1)
        take = []
        for k in range(2):
            code = table[:, k:k + 1].astype(jnp.int32) - 1
            code = (code >> 3) * (Y * CAP) + block * CAP + (code & 7)
            take.append((places == code).astype(jnp.float32).astype(jnp.bfloat16))
        at = pl.ds(p * Y * CAP, Y * CAP)
        arrived(recv_3.at[:, at], sem_3.at[p])
        source = recv_3[:, p * Y * CAP:(p + 1) * Y * CAP, :].reshape(EXPERTS * Y * CAP, half)
        total = 0.0
        for k in range(2):
            total = total + table[:, 2 + k:3 + k] * jnp.dot(take[k], source, preferred_element_type=jnp.float32)
        send_4[p * Y:(p + 1) * Y] = total.astype(jnp.bfloat16).reshape(Y, SLOTS, half)
        for dy in COLUMN:
            o = p * Y + dy
            remote(send_4.at[o], recv_4.at[o], s_sem.at[5], sem_4.at[p], plane(0, dy, -1), core).start()
        pltpu.make_async_copy(send_4.at[p * Y], recv_4.at[p * Y], sem_4.at[p]).start()

    def step_e(p):
        table = tables[p, 0, :, :2 * tokens]
        table = jnp.transpose(jnp.concatenate([table, jnp.zeros_like(table)], axis=0))
        spot = table[:tokens, 2:3].astype(jnp.int32) - p * Y * SLOTS
        places = lax.broadcasted_iota(jnp.int32, (tokens, Y * SLOTS), 1)
        take = (places == spot).astype(jnp.float32).astype(jnp.bfloat16)
        arrived(recv_4.at[pl.ds(p * Y, Y)], sem_4.at[p])
        source = recv_4[p * Y:(p + 1) * Y].reshape(Y * SLOTS, half)
        send_5[p] = jnp.dot(take, source, preferred_element_type=jnp.float32).astype(jnp.bfloat16)
        if p:
            remote(send_5.at[p], recv_5.at[p], s_sem.at[6], sem_5.at[p], plane(STEPS[p], 0, -1), core).start()
        else:
            pltpu.make_async_copy(send_5.at[0], recv_5.at[0], sem_5.at[0]).start()

    sums = []

    def step_h(p):
        arrived(recv_5.at[p], sem_5.at[p])
        sums.append(recv_5[p].astype(jnp.float32))

    step_of = {"G": step_g, "A": step_a, "F": step_f, "C": step_c, "E": step_e, "H": step_h}
    for name in ORDER.split():
        if name != "G00":
            step_of[name[0]](*map(int, name[1:]))
    out_ref[...] = sum(sums).astype(jnp.bfloat16)

    for at in ((pl.ds(1, Z - 1),), (0, pl.ds(1, X - 1))):
        arrived(tables.at[at], s_sem.at[0])
        arrived(blocks.at[at], s_sem.at[1])
    arrived(meta_r.at[pl.ds(1, OFFSETS - 1)], s_sem.at[2])
    arrived(recv_2.at[0, :, :, pl.ds(1, Y - 1)], s_sem.at[3])
    arrived(recv_2.at[1], s_sem.at[3])
    arrived(recv_3.at[pl.ds(1, EXPERTS - 1)], s_sem.at[4])
    arrived(send_4.at[pl.ds(0, OFFSETS - Z)], s_sem.at[5])
    arrived(send_5.at[pl.ds(1, Z - 1)], s_sem.at[6])


def solution(mesh):
    assert mesh.shape["ep"] == Z * Y * X and mesh.shape["tp"] == 2

    def local(tokens, norm_gain, routing, route_weight, w_gate, w_up, w_down):
        rows, half = tokens.shape
        vmem = pl.BlockSpec(memory_space=pltpu.VMEM)
        far = pl.BlockSpec(memory_space=pl.ANY)
        dma = pltpu.SemaphoreType.DMA
        bf16, f32 = jnp.bfloat16, jnp.float32
        line_rows = OFFSETS * CAP
        rounds = dma((Z,))
        return pl.pallas_call(
            kernel,
            out_shape=pltpu.VMEM((rows, half), bf16),
            in_specs=[far] * 7,
            out_specs=vmem,
            scratch_shapes=[
                pltpu.VMEM((2, rows), jnp.int32),
                pltpu.VMEM((2, rows), f32),
                pltpu.VMEM((2, 1, half), f32),
                pltpu.VMEM(w_gate.shape, bf16),
                pltpu.VMEM(w_up.shape, bf16),
                pltpu.VMEM(w_down.shape, bf16),
                pltpu.VMEM(w_gate.shape[1:], bf16),
                pltpu.VMEM(w_up.shape[1:], bf16),
                pltpu.VMEM(w_down.shape[1:], bf16),
                pltpu.VMEM((Z, 4, Y * SLOTS), f32),
                pltpu.VMEM((OFFSETS, 4, Y * SLOTS), f32),
                pltpu.VMEM((Z, X, rows, half), bf16),
                pltpu.VMEM((Z, X, 4, X * rows), f32),
                pltpu.VMEM((Z, Y, 2, X, CAP, half), bf16),
                pltpu.VMEM((2, Z, X, Y, CAP, half), bf16),
                pltpu.VMEM((X, 2, line_rows, half), bf16),
                pltpu.VMEM((EXPERTS, line_rows, half), bf16),
                pltpu.VMEM((OFFSETS, SLOTS, half), bf16),
                pltpu.VMEM((OFFSETS, SLOTS, half), bf16),
                pltpu.VMEM((Z, rows, half), bf16),
                pltpu.VMEM((Z, rows, half), bf16),
                dma((4,)), dma((3,)), dma((3,)), dma((4,)), dma((4,)), dma((7,)),
                rounds, dma((Z, X)), dma((Z, X)), rounds, rounds, rounds, rounds,
            ],
            compiler_params=pltpu.CompilerParams(collective_id=0, has_side_effects=True),
            name="experts",
        )(tokens, norm_gain.reshape(1, half), routing.T, route_weight.T, w_gate, w_up, w_down)

    in_specs = (
        P("ep", "tp"), P("tp"), P("ep", None), P("ep", None),
        P("ep", None, "tp"), P("ep", None, "tp"), P("ep", None, "tp"),
    )
    return jax.shard_map(local, mesh=mesh, in_specs=in_specs, out_specs=P("ep", "tp"), check_vma=False)
```

time: 74 us -> 70.7 us (0.955)
  Pallas kernels: 73.3 us -> 70 us
    pallas_call x1, Pallas kernels: 73.3 us -> 70 us  [local(): pl.pallas_call(kernel, out_shape=pltpu.VMEM((rows, half), bf16), in_specs...]
where the time goes in v3:
time: 70.7 us; the launch traced here: 70.6 us
  Pallas kernels  70 us (99%)
    pallas_call x1, Pallas kernels, local(): pl.pallas_call(kernel, out_shape=pltpu.VMEM((rows, half), bf16), in_specs...  70 us

profile of v3, /device:TPU:1, one launch (start us, length us, event | category | flops | bytes accessed | tf_op | source)
XLA Modules:
  0.0 70.6 jit_solution(6824997983364681309)
XLA Ops:
  0.0 70.0 %experts.1 = bf16[64,512]{1,0:T(8,128)(2,1)S(1)} custom-call(bf16[64,512]{1,0:T(8,128)(2,1)} %tok_hbm.1, f32[1,512]{1,0:T(1,128)} %bitcast.3, s32[2,64]{1,0:T(2,128)} %bitcast.4, f32[2,64]{1,0:T(2,128)} %bitcast.5, bf16[2,1024,256]{2,1,0:T(8,128)(2,1)} %wg_hbm.1, bf16[2,1024,256]{2,1,0:T(8,128)(2,1)} %wu_hbm.1, bf16[2,512,512]{2,1,0:T(8,128)(2,1)} %wd_hbm.1), custom_call_target="tpu_custom_call" | custom-call | tf_op jit(solution)/shard_map/experts/pallas_call | solution.py:318
  70.0 0.6 copy.9

commit v4 on v3

--- a/solution.py
+++ b/solution.py
@@ -17,10 +17,12 @@
 OFFSETS = Z * Y
 STEPS = (0, 1, 7, 2, 6, 3, 5, 4)
 LINE = (2, 1, 3)
+GATHER = (1, 3, 2)
 COLUMN = (2, 1, 3)
 ORDER = """
-    G00 G01 G03 G02 A0 G10 G11 G13 G12 A1 A2 G20 G21 F0 G23 G22 A3 A4 F1 G30 G31 C0 G33 G32 A5 A6 F2 F3 C1
-    A7 F4 C2 E0 F5 E1 C3 F6 E2 C4 F7 C5 E3 C6 E4 C7 E5 E6 E7 H0 H1 H2 H3 H4 H5 H6 H7
+    G00 G01 A00 G02 G03 G10 A01 A10 A20 G11 G12 A21 G13 A11 F0 A40 G21 A30 G20 A31 G23 F2 G22 A41 G30 A60 G31
+    A50 F3 G33 A61 A51 G32 F4 A70 F6 A71 C3 F5 C4 F7 C6 F1 E4 C5 C2 E3 E6 C7 E5 C1 H3 E7 C0 E2 E1 E0 H4 H0 H6 H2
+    H5 H1 H7
 """
 
 
@@ -107,12 +109,12 @@
         values = jnp.sum(jnp.where(at_home, columns[:, q + 1:q + 2], 0.0), axis=0, keepdims=True)
         for p in range(Z):
             meta_s[p, q:q + 1, :] = values[:, p * Y * SLOTS:(p + 1) * Y * SLOTS]
-    repeated = lax.broadcasted_iota(jnp.int32, (tokens, X * tokens), 1) % tokens
-    repeated = repeated == lax.broadcasted_iota(jnp.int32, (tokens, X * tokens), 0)
+    repeated = lax.broadcasted_iota(jnp.int32, (tokens, 2 * tokens), 1) % tokens
+    repeated = repeated == lax.broadcasted_iota(jnp.int32, (tokens, 2 * tokens), 0)
     for k in range(3):
         values = jnp.where(repeated, columns[:, 5 + k:6 + k], 0.0)
         tables[0, 0, k:k + 1, :] = jnp.sum(values, axis=0, keepdims=True)
-    tables[0, 0, 3:4, :] = jnp.zeros((1, X * tokens), jnp.float32)
+    tables[0, 0, 3:4, :] = jnp.zeros((1, 2 * tokens), jnp.float32)
     inputs[2].wait()
     inputs[3].wait()
 
@@ -150,7 +152,7 @@
             arrived(tables.at[p, j], table_sem.at[p, j])
             arrived(blocks.at[p, j], block_sem.at[p, j])
 
-    for dx in LINE:
+    for dx in GATHER:
         pass_on(0, 0, 0, dx, line(dx, 1))
     step_g(0, 0)
     pltpu.make_async_copy(meta_s.at[0], meta_r.at[0], meta_sem.at[0]).start()
@@ -178,32 +180,34 @@
             table = jnp.where(segment == dy, meta_r[p * Y + dy], table)
         return table
 
-    def step_a(p):
-        for j in range(X):
+    def step_a(p, h):
+        pair = X // 2
+        for j in range(h * pair, h * pair + pair):
             chunk_here(p, j)
-        spot_of = lax.broadcasted_iota(jnp.int32, (4, X * tokens), 1) // tokens
-        seat = jnp.zeros((4, X * tokens), jnp.float32)
-        for j in range(X):
-            seat = jnp.where(spot_of == j, tables[p, j], seat)
+        at = pl.ds(h * pair, pair)
+        spot_of = lax.broadcasted_iota(jnp.int32, (4, pair * tokens), 1) // tokens
+        seat = jnp.zeros((4, pair * tokens), jnp.float32)
+        for j in range(pair):
+            seat = jnp.where(spot_of == j, tables[p, h * pair + j, :, :pair * tokens], seat)
         seat = seat.astype(jnp.int32)
         pick = seat // CAP
         group, expert = pick // EXPERTS, pick % EXPERTS
         dy = (group % Y - y + Y) % Y
-        target = ((dy * 2 + expert % 2) * X + spot_of) * CAP + seat % CAP
+        target = ((dy * 2 + expert % 2) * pair + spot_of) * CAP + seat % CAP
         target = jnp.where((group // Y == z) & (expert // 2 == x), target, -1)
-        places = lax.broadcasted_iota(jnp.int32, (Y * 2 * X * CAP, X * tokens), 0)
+        places = lax.broadcasted_iota(jnp.int32, (Y * 2 * pair * CAP, pair * tokens), 0)
         take = (places == target[0:1]) | (places == target[1:2])
         take = take.astype(jnp.float32).astype(jnp.bfloat16)
-        source = blocks[p].reshape(X * tokens, half)
+        source = blocks[p, h * pair:h * pair + pair].reshape(pair * tokens, half)
         chosen = jnp.dot(take, source, preferred_element_type=jnp.float32)
-        send_2[p] = chosen.reshape(Y, 2, X, CAP, half).astype(jnp.bfloat16)
+        send_2[p, h] = chosen.reshape(Y, 2, pair, CAP, half).astype(jnp.bfloat16)
         for dy in COLUMN:
             for c in range(2):
                 remote(
-                    send_2.at[p, dy, c], recv_2.at[core, p, :, dy], s_sem.at[3], sem_2.at[p], plane(0, dy, 1), c
+                    send_2.at[p, h, dy, c], recv_2.at[core, p, at, dy], s_sem.at[3], sem_2.at[p], plane(0, dy, 1), c
                 ).start()
-        remote(send_2.at[p, 0, other], recv_2.at[core, p, :, 0], s_sem.at[3], sem_2.at[p], me, other).start()
-        pltpu.make_async_copy(send_2.at[p, 0, core], recv_2.at[core, p, :, 0], sem_2.at[p]).start()
+        remote(send_2.at[p, h, 0, other], recv_2.at[core, p, at, 0], s_sem.at[3], sem_2.at[p], me, other).start()
+        pltpu.make_async_copy(send_2.at[p, h, 0, core], recv_2.at[core, p, at, 0], sem_2.at[p]).start()
 
     ready = []
 
@@ -268,7 +272,7 @@
         pltpu.make_async_copy(send_4.at[p * Y], recv_4.at[p * Y], sem_4.at[p]).start()
 
     def step_e(p):
-        table = tables[p, 0, :, :2 * tokens]
+        table = tables[p, 0]
         table = jnp.transpose(jnp.concatenate([table, jnp.zeros_like(table)], axis=0))
         spot = table[:tokens, 2:3].astype(jnp.int32) - p * Y * SLOTS
         places = lax.broadcasted_iota(jnp.int32, (tokens, Y * SLOTS), 1)
@@ -333,8 +337,8 @@
                 pltpu.VMEM((Z, 4, Y * SLOTS), f32),
                 pltpu.VMEM((OFFSETS, 4, Y * SLOTS), f32),
                 pltpu.VMEM((Z, X, rows, half), bf16),
-                pltpu.VMEM((Z, X, 4, X * rows), f32),
-                pltpu.VMEM((Z, Y, 2, X, CAP, half), bf16),
+                pltpu.VMEM((Z, X, 4, 2 * rows), f32),
+                pltpu.VMEM((Z, 2, Y, 2, X // 2, CAP, half), bf16),
                 pltpu.VMEM((2, Z, X, Y, CAP, half), bf16),
                 pltpu.VMEM((X, 2, line_rows, half), bf16),
                 pltpu.VMEM((EXPERTS, line_rows, half), bf16),

time: 70.7 us -> 64.4 us (0.911)
  Pallas kernels: 70 us -> 63.7 us
    pallas_call x1, Pallas kernels: 70 us -> 63.7 us  [local(): pl.pallas_call(kernel, out_shape=pltpu.VMEM((rows, half), bf16), in_specs...]
where the time goes in v4:
time: 64.4 us; the launch traced here: 64.3 us
  Pallas kernels  63.7 us (99%)
    pallas_call x1, Pallas kernels, local(): pl.pallas_call(kernel, out_shape=pltpu.VMEM((rows, half), bf16), in_specs...  63.7 us

profile of v4, /device:TPU:1, one launch (start us, length us, event | category | flops | bytes accessed | tf_op | source)
XLA Modules:
  0.0 64.3 jit_solution(16827941368257126469)
XLA Ops:
  0.0 63.7 %experts.1 = bf16[64,512]{1,0:T(8,128)(2,1)S(1)} custom-call(bf16[64,512]{1,0:T(8,128)(2,1)} %tok_hbm.1, f32[1,512]{1,0:T(1,128)} %bitcast.3, s32[2,64]{1,0:T(2,128)} %bitcast.4, f32[2,64]{1,0:T(2,128)} %bitcast.5, bf16[2,1024,256]{2,1,0:T(8,128)(2,1)} %wg_hbm.1, bf16[2,1024,256]{2,1,0:T(8,128)(2,1)} %wu_hbm.1, bf16[2,512,512]{2,1,0:T(8,128)(2,1)} %wd_hbm.1), custom_call_target="tpu_custom_call" | custom-call | tf_op jit(solution)/shard_map/experts/pallas_call | solution.py:322
  63.7 0.6 copy.9

commit v5 on v4

--- a/solution.py
+++ b/solution.py
@@ -20,9 +20,9 @@
 GATHER = (1, 3, 2)
 COLUMN = (2, 1, 3)
 ORDER = """
-    G00 G01 A00 G02 G03 G10 A01 A10 A20 G11 G12 A21 G13 A11 F0 A40 G21 A30 G20 A31 G23 F2 G22 A41 G30 A60 G31
-    A50 F3 G33 A61 A51 G32 F4 A70 F6 A71 C3 F5 C4 F7 C6 F1 E4 C5 C2 E3 E6 C7 E5 C1 H3 E7 C0 E2 E1 E0 H4 H0 H6 H2
-    H5 H1 H7
+    G00 M0 G01 A00 G02 G03 G10 A01 A10 A20 G11 G12 A21 G13 A11 M1 M2 F0 A40 G21 A30 G20 A31 G23 F2 M3 M4 G22 A41
+    G30 A60 G31 A50 F3 G33 A61 A51 G32 F4 M5 M6 A70 F6 A71 M7 C3 F5 C4 F7 C6 F1 E4 C5 C2 E3 E6 C7 E5 C1 H3 E7 C0
+    E2 E1 E0 H4 H0 H6 H2 H5 H1 H7
 """
 
 
@@ -61,22 +61,11 @@
         copy.start()
 
     barrier = pltpu.get_barrier_semaphore()
-    greeted = 0
-    for step in STEPS:
-        for dy in range(Y):
-            if step or dy:
-                pl.semaphore_signal(barrier, inc=1, device_id=(plane(step, dy, 1), core), device_id_type=MESH)
-                greeted += 1
-    for dy in range(1, Y):
-        pl.semaphore_signal(barrier, inc=1, device_id=(plane(0, dy, 1), other), device_id_type=MESH)
-        greeted += 1
-    for dx in range(X):
-        for c in range(2):
-            if dx:
-                pl.semaphore_signal(barrier, inc=1, device_id=(line(dx, 1), c), device_id_type=MESH)
-                greeted += 1
-    pl.semaphore_signal(barrier, inc=1, device_id=(me, other), device_id_type=MESH)
-    greeted += 1
+    near = [(plane(step, 0, 1), core) for step in sorted({1, 2 % Z, Z - 2, Z - 1} - {0})] + [(me, other)]
+    near += [(plane(0, dy, 1), c) for dy in range(1, Y) for c in range(2)]
+    near += [(line(dx, 1), c) for dx in range(1, X) for c in range(2)]
+    for device in near:
+        pl.semaphore_signal(barrier, inc=1, device_id=device, device_id_type=MESH)
     for copy in give + own:
         copy.start()
 
@@ -118,7 +107,7 @@
     inputs[2].wait()
     inputs[3].wait()
 
-    pl.semaphore_wait(barrier, greeted)
+    pl.semaphore_wait(barrier, len(near))
 
     def remote(src, dst, send, recv, peer, c):
         return pltpu.make_async_remote_copy(
@@ -139,10 +128,15 @@
     def step_g(k, j):
         for p in sorted({place_of[k], place_of[(Z - k) % Z]}):
             chunk_here(p, j)
+        if (k, j) == (1, 0) and middle > 2:
+            return
         if k + 1 < middle or j < X // 2:
             pass_on(place_of[k], j, place_of[k + 1], j, up)
         if k + 1 < middle or j >= X // 2:
             pass_on(place_of[(Z - k) % Z], j, place_of[Z - k - 1], j, down)
+        if (k, j) == (0, 0) and middle > 2:
+            pass_on(0, 0, place_of[2], 0, plane(2, 0, 1))
+            pass_on(0, 0, place_of[Z - 2], 0, plane(2, 0, -1))
 
     seen = {(0, 0)}
 
@@ -155,12 +149,16 @@
     for dx in GATHER:
         pass_on(0, 0, 0, dx, line(dx, 1))
     step_g(0, 0)
-    pltpu.make_async_copy(meta_s.at[0], meta_r.at[0], meta_sem.at[0]).start()
-    for p, step in enumerate(STEPS):
+    def step_m(p):
+        assert (place_of[(Z - STEPS[p]) % Z], 0) in seen
         for dy in range(Y):
             if p or dy:
-                o, peer = p * Y + dy, plane(step, dy, 1)
+                o, peer = p * Y + dy, plane(STEPS[p], dy, 1)
                 remote(meta_s.at[p], meta_r.at[o], s_sem.at[2], meta_sem.at[p], peer, core).start()
+            else:
+                pltpu.make_async_copy(meta_s.at[0], meta_r.at[0], meta_sem.at[0]).start()
+
+    step_m(0)
 
     gain_copy = remote(gains.at[core], gains.at[core], far_send.at[3], far_recv.at[3], me, other)
     gain_copy.start()
@@ -285,17 +283,14 @@
         else:
             pltpu.make_async_copy(send_5.at[0], recv_5.at[0], sem_5.at[0]).start()
 
-    sums = []
-
     def step_h(p):
         arrived(recv_5.at[p], sem_5.at[p])
-        sums.append(recv_5[p].astype(jnp.float32))
-
-    step_of = {"G": step_g, "A": step_a, "F": step_f, "C": step_c, "E": step_e, "H": step_h}
+
+    step_of = {"G": step_g, "M": step_m, "A": step_a, "F": step_f, "C": step_c, "E": step_e, "H": step_h}
     for name in ORDER.split():
-        if name != "G00":
+        if name not in ("G00", "M0"):
             step_of[name[0]](*map(int, name[1:]))
-    out_ref[...] = sum(sums).astype(jnp.bfloat16)
+    out_ref[...] = sum(recv_5[p].astype(jnp.float32) for p in range(Z)).astype(jnp.bfloat16)
 
     for at in ((pl.ds(1, Z - 1),), (0, pl.ds(1, X - 1))):
         arrived(tables.at[at], s_sem.at[0])

time: 64.4 us -> 62.2 us (0.966)
  Pallas kernels: 63.7 us -> 61.5 us
    pallas_call x1, Pallas kernels: 63.7 us -> 61.5 us  [local(): pl.pallas_call(kernel, out_shape=pltpu.VMEM((rows, half), bf16), in_specs...]
where the time goes in v5:
time: 62.2 us; the launch traced here: 62.1 us
  Pallas kernels  61.5 us (99%)
  local copies, waits for them, and re-layouts  0.63 us (1%)
    pallas_call x1, Pallas kernels, local(): pl.pallas_call(kernel, out_shape=pltpu.VMEM((rows, half), bf16), in_specs...  61.5 us

profile of v5, /device:TPU:1, one launch (start us, length us, event | category | flops | bytes accessed | tf_op | source)
XLA Modules:
  0.0 62.1 jit_solution(11818029418318265281)
XLA Ops:
  0.0 61.5 %experts.1 = bf16[64,512]{1,0:T(8,128)(2,1)S(1)} custom-call(bf16[64,512]{1,0:T(8,128)(2,1)} %tok_hbm.1, f32[1,512]{1,0:T(1,128)} %bitcast.3, s32[2,64]{1,0:T(2,128)} %bitcast.4, f32[2,64]{1,0:T(2,128)} %bitcast.5, bf16[2,1024,256]{2,1,0:T(8,128)(2,1)} %wg_hbm.1, bf16[2,1024,256]{2,1,0:T(8,128)(2,1)} %wu_hbm.1, bf16[2,512,512]{2,1,0:T(8,128)(2,1)} %wd_hbm.1), custom_call_target="tpu_custom_call" | custom-call | tf_op jit(solution)/shard_map/experts/pallas_call | solution.py:317
  61.5 0.6 %copy.9 = bf16[64,512]{1,0:T(8,128)(2,1)} copy(bf16[64,512]{1,0:T(8,128)(2,1)S(1)} %experts.1) | data formatting | bytes 131072

commit v6 on v5

--- a/solution.py
+++ b/solution.py
@@ -16,13 +16,13 @@
 SLOTS = EXPERTS * CAP // 2
 OFFSETS = Z * Y
 STEPS = (0, 1, 7, 2, 6, 3, 5, 4)
-LINE = (2, 1, 3)
+LINE = (1, 3, 2)
 GATHER = (1, 3, 2)
 COLUMN = (2, 1, 3)
 ORDER = """
-    G00 M0 G01 A00 G02 G03 G10 A01 A10 A20 G11 G12 A21 G13 A11 M1 M2 F0 A40 G21 A30 G20 A31 G23 F2 M3 M4 G22 A41
-    G30 A60 G31 A50 F3 G33 A61 A51 G32 F4 M5 M6 A70 F6 A71 M7 C3 F5 C4 F7 C6 F1 E4 C5 C2 E3 E6 C7 E5 C1 H3 E7 C0
-    E2 E1 E0 H4 H0 H6 H2 H5 H1 H7
+    G00 A001 G01 A012 G02 G03 A201 G10 A101 A301 A401 M2 G11 A024 W G12 A112 A224 G13 A124 G20 G21 A312 A412 M1
+    F0 G22 A324 A212 G23 A424 F1 A501 M3 M4 A601 G30 A512 A612 G32 F3 A624 M6 M5 G33 G31 F4 M0 A524 A701 F6 A712
+    A724 F5 C3 C4 M7 C1 F7 C6 F2 C5 E4 E3 C0 E6 C7 E5 C2 E7 E2 E0 E1 H4 H3 H6 H0 H5 H2 H1 H7
 """
 
 
@@ -162,14 +162,16 @@
 
     gain_copy = remote(gains.at[core], gains.at[core], far_send.at[3], far_recv.at[3], me, other)
     gain_copy.start()
-    for copy in give:
-        copy.wait()
     far = [
         remote(stage, dst.at[core], far_send.at[i], far_recv.at[i], me, other)
         for i, (_, dst, stage) in enumerate(stores)
     ]
-    for copy in far:
-        copy.start()
+
+    def step_w():
+        for copy in give:
+            copy.wait()
+        for copy in far:
+            copy.start()
 
     def codes_of(p):
         segment = lax.broadcasted_iota(jnp.int32, (4, Y * SLOTS), 1) // SLOTS
@@ -178,34 +180,34 @@
             table = jnp.where(segment == dy, meta_r[p * Y + dy], table)
         return table
 
-    def step_a(p, h):
-        pair = X // 2
-        for j in range(h * pair, h * pair + pair):
+    def step_a(p, first, last):
+        count = last - first
+        for j in range(first, last):
             chunk_here(p, j)
-        at = pl.ds(h * pair, pair)
-        spot_of = lax.broadcasted_iota(jnp.int32, (4, pair * tokens), 1) // tokens
-        seat = jnp.zeros((4, pair * tokens), jnp.float32)
-        for j in range(pair):
-            seat = jnp.where(spot_of == j, tables[p, h * pair + j, :, :pair * tokens], seat)
+        at = pl.ds(first, count)
+        spot_of = lax.broadcasted_iota(jnp.int32, (4, count * tokens), 1) // tokens
+        seat = jnp.zeros((4, count * tokens), jnp.float32)
+        for j in range(count):
+            seat = jnp.where(spot_of == j, tables[p, first + j, :, :count * tokens], seat)
         seat = seat.astype(jnp.int32)
         pick = seat // CAP
         group, expert = pick // EXPERTS, pick % EXPERTS
         dy = (group % Y - y + Y) % Y
-        target = ((dy * 2 + expert % 2) * pair + spot_of) * CAP + seat % CAP
+        target = ((spot_of * Y + dy) * 2 + expert % 2) * CAP + seat % CAP
         target = jnp.where((group // Y == z) & (expert // 2 == x), target, -1)
-        places = lax.broadcasted_iota(jnp.int32, (Y * 2 * pair * CAP, pair * tokens), 0)
+        places = lax.broadcasted_iota(jnp.int32, (count * Y * 2 * CAP, count * tokens), 0)
         take = (places == target[0:1]) | (places == target[1:2])
         take = take.astype(jnp.float32).astype(jnp.bfloat16)
-        source = blocks[p, h * pair:h * pair + pair].reshape(pair * tokens, half)
+        source = blocks[p, first:last].reshape(count * tokens, half)
         chosen = jnp.dot(take, source, preferred_element_type=jnp.float32)
-        send_2[p, h] = chosen.reshape(Y, 2, pair, CAP, half).astype(jnp.bfloat16)
+        send_2[p, first:last] = chosen.reshape(count, Y, 2, CAP, half).astype(jnp.bfloat16)
         for dy in COLUMN:
             for c in range(2):
                 remote(
-                    send_2.at[p, h, dy, c], recv_2.at[core, p, at, dy], s_sem.at[3], sem_2.at[p], plane(0, dy, 1), c
+                    send_2.at[p, at, dy, c], recv_2.at[core, p, at, dy], s_sem.at[3], sem_2.at[p], plane(0, dy, 1), c
                 ).start()
-        remote(send_2.at[p, h, 0, other], recv_2.at[core, p, at, 0], s_sem.at[3], sem_2.at[p], me, other).start()
-        pltpu.make_async_copy(send_2.at[p, h, 0, core], recv_2.at[core, p, at, 0], sem_2.at[p]).start()
+        remote(send_2.at[p, at, 0, other], recv_2.at[core, p, at, 0], s_sem.at[3], sem_2.at[p], me, other).start()
+        pltpu.make_async_copy(send_2.at[p, at, 0, core], recv_2.at[core, p, at, 0], sem_2.at[p]).start()
 
     ready = []
 
@@ -283,14 +285,19 @@
         else:
             pltpu.make_async_copy(send_5.at[0], recv_5.at[0], sem_5.at[0]).start()
 
+    sums = []
+    last = int(ORDER.split()[-1][1:])
+
     def step_h(p):
+        if p == last:
+            sums.append(sum(recv_5[q].astype(jnp.float32) for q in range(Z) if q != last))
         arrived(recv_5.at[p], sem_5.at[p])
 
-    step_of = {"G": step_g, "M": step_m, "A": step_a, "F": step_f, "C": step_c, "E": step_e, "H": step_h}
+    step_of = {"W": step_w, "G": step_g, "M": step_m, "A": step_a, "F": step_f, "C": step_c, "E": step_e, "H": step_h}
     for name in ORDER.split():
         if name not in ("G00", "M0"):
             step_of[name[0]](*map(int, name[1:]))
-    out_ref[...] = sum(recv_5[p].astype(jnp.float32) for p in range(Z)).astype(jnp.bfloat16)
+    out_ref[...] = (sums[0] + recv_5[last].astype(jnp.float32)).astype(jnp.bfloat16)
 
     for at in ((pl.ds(1, Z - 1),), (0, pl.ds(1, X - 1))):
         arrived(tables.at[at], s_sem.at[0])
@@ -333,7 +340,7 @@
                 pltpu.VMEM((OFFSETS, 4, Y * SLOTS), f32),
                 pltpu.VMEM((Z, X, rows, half), bf16),
                 pltpu.VMEM((Z, X, 4, 2 * rows), f32),
-                pltpu.VMEM((Z, 2, Y, 2, X // 2, CAP, half), bf16),
+                pltpu.VMEM((Z, X, Y, 2, CAP, half), bf16),
                 pltpu.VMEM((2, Z, X, Y, CAP, half), bf16),
                 pltpu.VMEM((X, 2, line_rows, half), bf16),
                 pltpu.VMEM((EXPERTS, line_rows, half), bf16),

time: 62.2 us -> 62.5 us (level)
  no operation moved by 1% of the time
where the time goes in v6:
time: 62.5 us; the launch traced here: 62.4 us
  Pallas kernels  61.7 us (99%)
  local copies, waits for them, and re-layouts  0.63 us (1%)
    pallas_call x1, Pallas kernels, local(): pl.pallas_call(kernel, out_shape=pltpu.VMEM((rows, half), bf16), in_specs...  61.7 us

profile of v6, /device:TPU:1, one launch (start us, length us, event | category | flops | bytes accessed | tf_op | source)
XLA Modules:
  0.0 62.4 jit_solution(17160202684513146756)
XLA Ops:
  0.0 61.7 %experts.1 = bf16[64,512]{1,0:T(8,128)(2,1)S(1)} custom-call(bf16[64,512]{1,0:T(8,128)(2,1)} %tok_hbm.1, f32[1,512]{1,0:T(1,128)} %bitcast.3, s32[2,64]{1,0:T(2,128)} %bitcast.4, f32[2,64]{1,0:T(2,128)} %bitcast.5, bf16[2,1024,256]{2,1,0:T(8,128)(2,1)} %wg_hbm.1, bf16[2,1024,256]{2,1,0:T(8,128)(2,1)} %wu_hbm.1, bf16[2,512,512]{2,1,0:T(8,128)(2,1)} %wd_hbm.1), custom_call_target="tpu_custom_call" | custom-call | tf_op jit(solution)/shard_map/experts/pallas_call | solution.py:324
  61.8 0.6 %copy.9 = bf16[64,512]{1,0:T(8,128)(2,1)} copy(bf16[64,512]{1,0:T(8,128)(2,1)S(1)} %experts.1) | data formatting | bytes 131072

commit v7 on v5

--- a/solution.py
+++ b/solution.py
@@ -19,11 +19,13 @@
 LINE = (2, 1, 3)
 GATHER = (1, 3, 2)
 COLUMN = (2, 1, 3)
-ORDER = """
-    G00 M0 G01 A00 G02 G03 G10 A01 A10 A20 G11 G12 A21 G13 A11 M1 M2 F0 A40 G21 A30 G20 A31 G23 F2 M3 M4 G22 A41
-    G30 A60 G31 A50 F3 G33 A61 A51 G32 F4 M5 M6 A70 F6 A71 M7 C3 F5 C4 F7 C6 F1 E4 C5 C2 E3 E6 C7 E5 C1 H3 E7 C0
-    E2 E1 E0 H4 H0 H6 H2 H5 H1 H7
-"""
+ORDER = (
+    "G00", "M0", "G01", "A00", "G02", "G03", "G10", "A01", "A10", "A20", "G11", "G12", "A21", "G13", "A11",
+    "M1", "M2", "F0", "A40", "G21", "A30", "G20", "A31", "G23", "F2", "M3", "M4", "G22", "A41", "G30", "A60",
+    "G31", "A50", "F3", "G33", "A61", "A51", "G32", "F4", "M5", "M6", "A70", "F6", "A71", "M7", "C3", "F5",
+    "C4", "F7", "C6", "F1", "E4", "C5", "C2", "E3", "E6", "C7", "E5", "C1", "H3", "E7", "C0", "E2", "E1", "E0",
+    "H4", "H0", "H6", "H2", "H5", "H1", "H7",
+)
 
 
 def kernel(
@@ -287,7 +289,7 @@
         arrived(recv_5.at[p], sem_5.at[p])
 
     step_of = {"G": step_g, "M": step_m, "A": step_a, "F": step_f, "C": step_c, "E": step_e, "H": step_h}
-    for name in ORDER.split():
+    for name in ORDER:
         if name not in ("G00", "M0"):
             step_of[name[0]](*map(int, name[1:]))
     out_ref[...] = sum(recv_5[p].astype(jnp.float32) for p in range(Z)).astype(jnp.bfloat16)

time: 62.2 us -> 62.2 us (level)
  no operation moved by 1% of the time
where the time goes in v7:
time: 62.2 us; the launch traced here: 62.1 us
  Pallas kernels  61.5 us (99%)
  local copies, waits for them, and re-layouts  0.63 us (1%)
    pallas_call x1, Pallas kernels, local(): pl.pallas_call(kernel, out_shape=pltpu.VMEM((rows, half), bf16), in_specs...  61.5 us

profile of v7, /device:TPU:1, one launch (start us, length us, event | category | flops | bytes accessed | tf_op | source)
XLA Modules:
  0.0 62.1 jit_solution(11818029418318265281)
XLA Ops:
  0.0 61.5 %experts.1 = bf16[64,512]{1,0:T(8,128)(2,1)S(1)} custom-call(bf16[64,512]{1,0:T(8,128)(2,1)} %tok_hbm.1, f32[1,512]{1,0:T(1,128)} %bitcast.3, s32[2,64]{1,0:T(2,128)} %bitcast.4, f32[2,64]{1,0:T(2,128)} %bitcast.5, bf16[2,1024,256]{2,1,0:T(8,128)(2,1)} %wg_hbm.1, bf16[2,1024,256]{2,1,0:T(8,128)(2,1)} %wu_hbm.1, bf16[2,512,512]{2,1,0:T(8,128)(2,1)} %wd_hbm.1), custom_call_target="tpu_custom_call" | custom-call | tf_op jit(solution)/shard_map/experts/pallas_call | solution.py:319
  61.5 0.6 %copy.9 = bf16[64,512]{1,0:T(8,128)(2,1)} copy(bf16[64,512]{1,0:T(8,128)(2,1)S(1)} %experts.1) | data formatting | bytes 131072

commit v8 on v6

--- a/solution.py
+++ b/solution.py
@@ -19,11 +19,14 @@
 LINE = (1, 3, 2)
 GATHER = (1, 3, 2)
 COLUMN = (2, 1, 3)
-ORDER = """
-    G00 A001 G01 A012 G02 G03 A201 G10 A101 A301 A401 M2 G11 A024 W G12 A112 A224 G13 A124 G20 G21 A312 A412 M1
-    F0 G22 A324 A212 G23 A424 F1 A501 M3 M4 A601 G30 A512 A612 G32 F3 A624 M6 M5 G33 G31 F4 M0 A524 A701 F6 A712
-    A724 F5 C3 C4 M7 C1 F7 C6 F2 C5 E4 E3 C0 E6 C7 E5 C2 E7 E2 E0 E1 H4 H3 H6 H0 H5 H2 H1 H7
-"""
+ORDER = (
+    "G00", "A001", "G01", "A012", "G02", "G03", "A201", "G10", "A101", "A301", "A401", "M2", "G11", "A024",
+    "G12", "A112", "A224", "G13", "A124", "G20", "G21", "A312", "A412", "M1", "F0", "G22", "A324", "A212",
+    "G23", "A424", "F1", "A501", "M3", "M4", "A601", "G30", "A512", "A612", "G32", "F3", "A624", "M6", "M5",
+    "G33", "G31", "F4", "M0", "A524", "A701", "F6", "A712", "A724", "F5", "C3", "C4", "M7", "C1", "F7", "C6",
+    "F2", "C5", "E4", "E3", "C0", "E6", "C7", "E5", "C2", "E7", "E2", "E0", "E1", "H4", "H3", "H6", "H0", "H5",
+    "H2", "H1", "H7",
+)
 
 
 def kernel(
@@ -162,16 +165,14 @@
 
     gain_copy = remote(gains.at[core], gains.at[core], far_send.at[3], far_recv.at[3], me, other)
     gain_copy.start()
+    for copy in give:
+        copy.wait()
     far = [
         remote(stage, dst.at[core], far_send.at[i], far_recv.at[i], me, other)
         for i, (_, dst, stage) in enumerate(stores)
     ]
-
-    def step_w():
-        for copy in give:
-            copy.wait()
-        for copy in far:
-            copy.start()
+    for copy in far:
+        copy.start()
 
     def codes_of(p):
         segment = lax.broadcasted_iota(jnp.int32, (4, Y * SLOTS), 1) // SLOTS
@@ -286,15 +287,15 @@
             pltpu.make_async_copy(send_5.at[0], recv_5.at[0], sem_5.at[0]).start()
 
     sums = []
-    last = int(ORDER.split()[-1][1:])
+    last = int(ORDER[-1][1:])
 
     def step_h(p):
         if p == last:
             sums.append(sum(recv_5[q].astype(jnp.float32) for q in range(Z) if q != last))
         arrived(recv_5.at[p], sem_5.at[p])
 
-    step_of = {"W": step_w, "G": step_g, "M": step_m, "A": step_a, "F": step_f, "C": step_c, "E": step_e, "H": step_h}
-    for name in ORDER.split():
+    step_of = {"G": step_g, "M": step_m, "A": step_a, "F": step_f, "C": step_c, "E": step_e, "H": step_h}
+    for name in ORDER:
         if name not in ("G00", "M0"):
             step_of[name[0]](*map(int, name[1:]))
     out_ref[...] = (sums[0] + recv_5[last].astype(jnp.float32)).astype(jnp.bfloat16)

time: 62.5 us -> 62.6 us (level)
  no operation moved by 1% of the time
where the time goes in v8:
time: 62.6 us; the launch traced here: 62.5 us
  Pallas kernels  61.9 us (99%)
  local copies, waits for them, and re-layouts  0.63 us (1%)
    pallas_call x1, Pallas kernels, local(): pl.pallas_call(kernel, out_shape=pltpu.VMEM((rows, half), bf16), in_specs...  61.9 us

profile of v8, /device:TPU:1, one launch (start us, length us, event | category | flops | bytes accessed | tf_op | source)
XLA Modules:
  0.0 62.5 jit_solution(12771104988042254906)
XLA Ops:
  0.0 61.9 %experts.1 = bf16[64,512]{1,0:T(8,128)(2,1)S(1)} custom-call(bf16[64,512]{1,0:T(8,128)(2,1)} %tok_hbm.1, f32[1,512]{1,0:T(1,128)} %bitcast.3, s32[2,64]{1,0:T(2,128)} %bitcast.4, f32[2,64]{1,0:T(2,128)} %bitcast.5, bf16[2,1024,256]{2,1,0:T(8,128)(2,1)} %wg_hbm.1, bf16[2,1024,256]{2,1,0:T(8,128)(2,1)} %wu_hbm.1, bf16[2,512,512]{2,1,0:T(8,128)(2,1)} %wd_hbm.1), custom_call_target="tpu_custom_call" | custom-call | tf_op jit(solution)/shard_map/experts/pallas_call | solution.py:325
  61.9 0.6 %copy.9 = bf16[64,512]{1,0:T(8,128)(2,1)} copy(bf16[64,512]{1,0:T(8,128)(2,1)S(1)} %experts.1) | data formatting | bytes 131072
